TPU v7x, 32 devices: a whole 2x2x4 slice. The times are simulated.
32 devices in a mesh: sp: 8 (over z, core), tp: 4 (over y, x).
Axes of the slice: x: 2, y: 2, z: 4, core: 2. Of those that a mesh axis runs over, the one named last changes fastest.
Arguments:
- residual: bfloat16 [1024, 4096], P('sp', 'tp'), may hold values from -46 to 46
- query_small: bfloat16 [1024, 2048], P('sp', 'tp'), may hold values from -6 to 6
- key_narrow_group: bfloat16 [1024, 2048], P('sp', 'tp'), may hold values from -6 to 6
- query_large: bfloat16 [1024, 4096], P('sp', 'tp'), may hold values from -6 to 6
- key_large: bfloat16 [1024, 4096], P('sp', 'tp'), may hold values from -6 to 6
- values: bfloat16 [1024, 2, 2048], P('sp', None, 'tp'), may hold values from -6 to 6
- gates: bfloat16 [1024, 2, 2048], P('sp', None, 'tp'), may hold values from -6 to 6
- log_decay: float32 [1024, 2, 16], P('sp', None, 'tp'), may hold values from -0.65 to 0, as said below
- head_gain: float32 [2, 2048], P(None, 'tp'), may hold values from 0.1 to 1.9
- out_weight: bfloat16 [2, 2048, 4096], P(None, 'sp', 'tp'), may hold values from -0.09375 to 0.09375
- norm_gain: float32 [4096], P('tp'), may hold values from 0.1 to 1.9
- routes: int32 [1024, 2], P('sp'), may hold values from 0 to 7, all different within a row; in each aligned block of 128 rows (0 to 127, 128 to 255, ...) at most 64 rows name the same one
- route_weight: float32 [1024, 2], P('sp'), may hold values from 0.2 to 1
- expert_gate: bfloat16 [8, 4096, 2048], P('sp', None, 'tp'), may hold values from -0.09375 to 0.09375
- expert_up: bfloat16 [8, 4096, 2048], P('sp', None, 'tp'), may hold values from -0.09375 to 0.09375
- expert_down: bfloat16 [8, 2048, 4096], P('sp', None, 'tp'), may hold values from -0.5 to 0.5
Outputs:
- new_stream: bfloat16 [1024, 4096], P('sp', 'tp')
Inputs may be any that keep to these rules, and one draw needn't show every extreme that they name: `routes`: each row names two different experts; in each aligned block of 128 rows no expert is named more than 64 times, a bound that some block reaches. `log_decay`: negative at every position.
All inputs are finite; a program needn't handle non-finite values.
Results may differ from a plain program's by a relative error of at most 0.019.
Values may be sent and summed in bfloat16 or wider, within the bound.
A program may use at most 64 MiB of HBM per device.

v0:
```python
import jax
import jax.numpy as jnp
from jax import lax
from jax.sharding import PartitionSpec as P

D = 4096


EPS = 1e-06
THETA = 10000.0


def entering_2(array, axis, combine, identity):
    devices, place = (lax.axis_size(axis), lax.axis_index(axis))
    everything = jax.tree.map(lambda part: lax.all_gather(part, axis), array)
    start = jax.tree.map(
        lambda part, zero: jnp.broadcast_to(jnp.asarray(zero, part.dtype), part.shape),
        array,
        identity,
    )

    def step(k, before):
        reached = k < place
        new = combine(before, jax.tree.map(lambda part: part[k], everything))
        return jax.tree.map(lambda a, b: jnp.where(reached, a, b), new, before)

    return lax.fori_loop(0, devices, step, start)


def rotate(block, positions):
    half_dim = block.shape[-1] // 2
    inverse = jnp.power(THETA, -jnp.arange(half_dim, dtype=jnp.float32) * 2.0 / block.shape[-1])
    angles = positions[:, None, None] * inverse
    cosine_val, sine_val = (jnp.cos(angles), jnp.sin(angles))
    lower_half, upper_half = (block[..., :half_dim], block[..., half_dim:])
    return jnp.concatenate(
        [
            lower_half * cosine_val - upper_half * sine_val,
            upper_half * cosine_val + lower_half * sine_val,
        ],
        axis=-1,
    )


def block_terms(rot_queries, rot_keys, value_heads, rates):
    count = rates.shape[0]
    decay_sum = jnp.cumsum(rates, axis=0)
    by_head = decay_sum.T
    causal = (jnp.arange(count)[:, None] >= jnp.arange(count)[None, :])[None]
    spread = by_head[:, :, None] - by_head[:, None, :]
    weight = jnp.where(causal, jnp.exp(jnp.where(causal, spread, 0.0)), 0.0)
    scores = jnp.einsum("ihd,jhd->hij", rot_queries, rot_keys, preferred_element_type=jnp.float32)
    weighted = (scores * weight).astype(jnp.bfloat16)
    within = jnp.einsum("hij,jhv->ihv", weighted, value_heads, preferred_element_type=jnp.float32)
    block_end = decay_sum[-1]
    carried = (
        rot_keys.astype(jnp.float32) * jnp.exp(block_end[None, :] - decay_sum)[:, :, None]
    ).astype(jnp.bfloat16)
    update = jnp.einsum("jhd,jhv->hdv", carried, value_heads, preferred_element_type=jnp.float32)
    return (within, decay_sum, jnp.exp(block_end), update)


def final_result(rot_queries, decay_sum, within, state_in, gate_part, gain_part):
    cross_part = (
        jnp.einsum(
            "ihd,hdv->ihv",
            rot_queries.astype(jnp.float32),
            state_in,
            precision=lax.Precision.HIGHEST,
        )
        * jnp.exp(decay_sum)[:, :, None]
    )
    retained = within + cross_part
    scaled = retained * lax.rsqrt(jnp.mean(retained * retained, axis=-1, keepdims=True) + EPS)
    count, head_count, value_size = retained.shape
    gated = jax.nn.silu(gate_part.astype(jnp.float32)).reshape(count, head_count, value_size)
    return (
        (scaled * gain_part.reshape(head_count, value_size) * gated)
        .reshape(count, -1)
        .astype(jnp.bfloat16)
    )


def prepare(queries, keys_in, value_part, positions, head_count):
    row_count = queries.shape[0]
    key_size = queries.shape[1] // head_count
    rot_queries = rotate(
        queries.astype(jnp.float32).reshape(row_count, head_count, key_size), positions
    ).astype(jnp.bfloat16)
    rot_keys = (
        rotate(keys_in.astype(jnp.float32).reshape(row_count, head_count, key_size), positions)
        * key_size ** (-0.5)
    ).astype(jnp.bfloat16)
    value_heads = value_part.reshape(row_count, head_count, value_part.shape[1] // head_count)
    return (rot_queries, rot_keys, value_heads)


def per_device(
    residual,
    query_small,
    key_narrow_group,
    query_large,
    key_large,
    values,
    gates,
    log_decay,
    head_gain,
    out_weight,
    norm_gain,
    routes,
    route_weight,
    expert_gate,
    expert_up,
    expert_down,
):
    row_count = residual.shape[0]
    head_count = log_decay.shape[2]
    positions = (lax.axis_index("sp") * row_count + jnp.arange(row_count, dtype=jnp.int32)).astype(
        jnp.float32
    )
    query_a, key_a, value_a = prepare(
        query_small, key_narrow_group, values[:, 0], positions, head_count
    )
    query_b, key_b, value_b = prepare(query_large, key_large, values[:, 1], positions, head_count)
    within_a, decay_sum_a, fall_a, update_a = block_terms(query_a, key_a, value_a, log_decay[:, 0])
    within_b, decay_sum_b, fall_b, update_b = block_terms(query_b, key_b, value_b, log_decay[:, 1])

    def combine(before_part, after_part):
        return (
            before_part[0] * after_part[0],
            after_part[0][:, None, None] * before_part[1] + after_part[1],
            before_part[2] * after_part[2],
            after_part[2][:, None, None] * before_part[3] + after_part[3],
        )

    identity = (
        jnp.ones_like(fall_a),
        jnp.zeros_like(update_a),
        jnp.ones_like(fall_b),
        jnp.zeros_like(update_b),
    )
    entering = entering_2((fall_a, update_a, fall_b, update_b), "sp", combine, identity)
    output_a = final_result(query_a, decay_sum_a, within_a, entering[1], gates[:, 0], head_gain[0])
    output_b = final_result(query_b, decay_sum_b, within_b, entering[3], gates[:, 1], head_gain[1])
    stacked = jnp.stack([output_a, output_b], axis=1)
    gathered = lax.all_gather(stacked, "tp", axis=2, tiled=True)
    mixed = jnp.einsum(
        "tgk,gkd->td",
        gathered,
        lax.all_gather(out_weight, "sp", axis=1, tiled=True),
        preferred_element_type=jnp.float32,
    ).astype(jnp.bfloat16)
    stream = residual.astype(jnp.float32) + mixed.astype(jnp.float32)
    square_sum = lax.psum(jnp.sum(stream * stream, axis=1), "tp")
    normed = (stream * lax.rsqrt(square_sum / D + EPS)[:, None] * norm_gain[None, :]).astype(
        jnp.bfloat16
    )
    experts = lax.axis_size("sp")
    capacity = 4 * row_count // experts
    one_hot = (routes[:, :, None] == jnp.arange(experts, dtype=jnp.int32)[None, None, :]).astype(
        jnp.int32
    )
    one_hot = one_hot.reshape(2 * row_count, experts)
    before = jnp.cumsum(one_hot, axis=0) - one_hot
    slot_index = jnp.sum(before * one_hot, axis=1).reshape(row_count, 2)
    target = routes * capacity + slot_index
    slot_ids = jnp.arange(experts * capacity, dtype=jnp.int32)
    choose = target[:, :, None] == slot_ids[None, None, :]
    select = jnp.sum(choose.astype(jnp.int32), axis=1).astype(jnp.bfloat16).T
    w_gate, w_up, w_down = (expert_gate[0], expert_up[0], expert_down[0])
    outgoing = jnp.dot(select, normed, preferred_element_type=jnp.float32).astype(jnp.bfloat16)
    outgoing = outgoing.reshape(experts, capacity, normed.shape[1])
    arrived = lax.all_to_all(outgoing, "sp", split_axis=0, concat_axis=0, tiled=True)
    expert_arrived = lax.all_gather(arrived, "tp", axis=2, tiled=True)
    gate_part = jnp.einsum(
        "sck,kf->scf", expert_arrived, w_gate, preferred_element_type=jnp.float32
    )
    up_part = jnp.einsum("sck,kf->scf", expert_arrived, w_up, preferred_element_type=jnp.float32)
    hidden = (jax.nn.silu(gate_part) * up_part).astype(jnp.bfloat16)
    expert_out = jnp.einsum(
        "scf,fd->scd",
        lax.all_gather(hidden, "tp", axis=2, tiled=True),
        w_down,
        preferred_element_type=jnp.float32,
    ).astype(jnp.bfloat16)
    returned = lax.all_to_all(expert_out, "sp", split_axis=0, concat_axis=0, tiled=True).reshape(
        experts * capacity, -1
    )
    first_pick = jnp.dot(
        choose[:, 0].astype(jnp.bfloat16), returned, preferred_element_type=jnp.float32
    )
    second_pick = jnp.dot(
        choose[:, 1].astype(jnp.bfloat16), returned, preferred_element_type=jnp.float32
    )
    routed = route_weight[:, 0:1] * first_pick + route_weight[:, 1:2] * second_pick
    return (stream + routed).astype(jnp.bfloat16)


def solution(mesh):
    placed = (
        P("sp", "tp"),
        P("sp", "tp"),
        P("sp", "tp"),
        P("sp", "tp"),
        P("sp", "tp"),
        P("sp", None, "tp"),
        P("sp", None, "tp"),
        P("sp", None, "tp"),
        P(None, "tp"),
        P(None, "sp", "tp"),
        P("tp"),
        P("sp", None),
        P("sp", None),
        P("sp", None, "tp"),
        P("sp", None, "tp"),
        P("sp", None, "tp"),
    )
    return jax.shard_map(
        per_device, mesh=mesh, in_specs=placed, out_specs=P("sp", "tp"), check_vma=False
    )
```

profile of v0, /device:TPU:0, one launch (start us, length us, event | category | flops | bytes accessed | tf_op | source)
XLA Modules:
  0.0 408.3 jit_solution(11339238263994428955)
XLA Ops:
  7.3 1.5 fusion.79
  15.9 1.2 fusion.32
  18.2 13.6 %all-gather.3 = f32[8,1,4]{2,1,0:T(1,128)S(1)} all-gather(f32[1,1,4]{2,1,0:T(1,128)S(1)} %get-tuple-element.253), channel_id=1, replica_groups=mesh['sp'=8,'tp'=4] {'sp'}, dimensions={0}, use_global_device_ids=true | all-gather | bytes 144 | tf_op jit(solution)/shard_map/all_gather | solution.py:15
  31.8 9.0 %all-gather.2 = f32[8,1,4]{2,1,0:T(1,128)S(1)} all-gather(f32[1,1,4]{2,1,0:T(1,128)S(1)} %get-tuple-element.255), channel_id=1, replica_groups=mesh['sp'=8,'tp'=4] {'sp'}, dimensions={0}, use_global_device_ids=true | all-gather | bytes 144 | tf_op jit(solution)/shard_map/all_gather | solution.py:15
  41.3 4.5 %all-gather.19.cloned.1.call-done = f32[32,128,128]{2,1,0:T(8,128)} async-done(((f32[4,128,128]{2,1,0:T(8,128)}), f32[32,128,128]{2,1,0:T(8,128)}) %all-gather.19.cloned.1.call-update) | async-done | bytes 2097168 | tf_op jit(solution)/shard_map/all_gather | solution.py:15
  45.8 47.9 %all-gather.21.cloned.1.call-done = f32[32,256,128]{2,1,0:T(8,128)} async-done(((f32[4,256,128]{2,1,0:T(8,128)}), f32[32,256,128]{2,1,0:T(8,128)}) %all-gather.21.cloned.1.call-update) | async-done | bytes 4194320 | tf_op jit(solution)/shard_map/all_gather | solution.py:15
  93.7 18.1 %while.16 = (s32[]{:T(128)}, f32[4,128,128]{2,1,0:T(8,128)S(1)}, f32[4,256,128]{2,1,0:T(8,128)S(1)}, s32[]{:T(128)}, f32[8,4]{1,0:T(8,128)S(1)}, /*index=5*/f32[...) while((s32[]{:T(128)}, f32[4,128,128]{2,1,0:T(8,128)S(1)}, ...), condition=%wide.region_3.4_spmd.clone, body=%wide.region_2.3_spmd.clone.sunk | while | flops 786436 | bytes 2359527 | solution.py:27
  96.0 1.2 fusion.106
  98.2 1.2 fusion.106
  102.8 1.2 fusion.106
  105.1 1.2 fusion.106
  109.6 1.2 fusion.106
  117.0 23.0 %all-gather.11.cloned.1.call-done = bf16[128,2,2048]{2,0,1:T(8,128)(2,1)} async-done(((bf16[128,2,512]{2,0,1:T(8,128)(2,1)}), bf16[128,2,2048]{2,0,1:T(8,128)(2,1)}) %all-gather.11.cloned.1.call-update) | async-done | bytes 1048592 | tf_op jit(solution)/shard_map/all_gather | solution.py:146
  140.0 83.5 %all-gather.13.cloned.1.call-done = bf16[2,2048,1024]{2,1,0:T(8,128)(2,1)} async-done(((bf16[2,256,1024]{2,1,0:T(8,128)(2,1)}), bf16[2,2048,1024]{2,1,0:T(8,128)(2,1)}) %all-gather.13.cloned.1.call-update) | async-done | bytes 8388624 | tf_op jit(solution)/shard_map/all_gather | solution.py:150
  223.6 5.1 %multiply_reduce_fusion = (f32[128]{0:T(128)S(1)}, f32[128,1024]{1,0:T(8,128)S(1)}) fusion(bf16[128,2,2048]{2,0,1:T(8,128)(2,1)} %all-gather.11.cloned.1.call-done, bf16[2,2048,1024]{2,1,0:T(8,128)(2,1)} %all-gather.13.cloned.1.call-done, bf16[128,1024]{1,0:T(8,128)(2,1)S(1)} %copy-done.1), kind=kOutput, calls=%fused_computation.42 | convolution fusion | flops 1074528128 | bytes 10224128 | tf_op jit(solution)/shard_map/tgk,gkd->td/dot_general | solution.py:147
  228.6 9.8 %psum.7 = f32[128]{0:T(128)S(1)} all-reduce(f32[128]{0:T(128)S(1)} %get-tuple-element.270), channel_id=1, replica_groups=mesh['sp'=8,'tp'=4] {'tp'}, use_global_device_ids=true, to_apply=%region_11.12 | all-reduce | flops 128 | bytes 1024 | tf_op jit(solution)/shard_map/psum | solution.py:154
  239.0 29.7 %all_to_all.10 = bf16[8,64,1024]{2,1,0:T(8,128)(2,1)} all-to-all(bf16[8,64,1024]{2,1,0:T(8,128)(2,1)S(1)} %bitcast.130), channel_id=1, replica_groups=mesh['sp'=8,'tp'=4] {'sp'}, dimensions={0} | all-to-all | bytes 2097152 | tf_op jit(solution)/shard_map/all_to_all | solution.py:173
  268.9 49.5 %all-gather.15.cloned.1.call-done = bf16[8,64,4096]{2,1,0:T(8,128)(2,1)} async-done(((bf16[8,64,1024]{2,1,0:T(8,128)(2,1)}), bf16[8,64,4096]{2,1,0:T(8,128)(2,1)}) %all-gather.15.cloned.1.call-update) | async-done | bytes 4194320 | tf_op jit(solution)/shard_map/all_gather | solution.py:174
  318.5 5.9 %fusion.8 = f32[8,64,512]{2,1,0:T(8,128)S(1)} fusion(bf16[8,64,4096]{2,1,0:T(8,128)(2,1)} %all-gather.15.cloned.1.call-done, bf16[1,4096,512]{2,1,0:T(8,128)(2,1)} %param.31), kind=kOutput, calls=%fused_computation.12 | convolution fusion | flops 2147483648 | bytes 9437184 | tf_op jit(solution)/shard_map/sck,kf->scf/dot_general | solution.py:175
  324.4 3.2 fusion.16
  327.7 35.2 %all-gather.17.cloned.1.call-done = bf16[8,64,2048]{2,1,0:T(8,128)(2,1)} async-done(((bf16[8,64,512]{2,1,0:T(8,128)(2,1)}), bf16[8,64,2048]{2,1,0:T(8,128)(2,1)}) %all-gather.17.cloned.1.call-update) | async-done | bytes 2097168 | tf_op jit(solution)/shard_map/all_gather | solution.py:182
  362.8 6.1 %fusion.10 = bf16[8,64,1024]{2,1,0:T(8,128)(2,1)} fusion(bf16[8,64,2048]{2,1,0:T(8,128)(2,1)} %all-gather.17.cloned.1.call-done, bf16[1,2048,1024]{2,1,0:T(8,128)(2,1)} %param.33), kind=kOutput, calls=%fused_computation.15 | convolution fusion | flops 2148007936 | bytes 7340032 | tf_op jit(solution)/shard_map/scf,fd->scd/dot_general | solution.py:180
  369.0 4.6 %all-to-all-start.1 = ((bf16[8,64,1024]{2,1,0:T(8,128)(2,1)}), bf16[8,64,1024]{2,1,0:T(8,128)(2,1)S(1)}, u32[]{:S(2)}, u32[]{:S(2)}) async-start(bf16[8,64,1024]{2,1,0:T(8,128)(2,1)} %fusion.10), calls=%async_computation.1 | async-start | bytes 2097152 | tf_op jit(solution)/shard_map/all_to_all | solution.py:186
  373.7 26.4 %all-to-all-done.1 = bf16[8,64,1024]{2,1,0:T(8,128)(2,1)S(1)} async-done(((bf16[8,64,1024]{2,1,0:T(8,128)(2,1)}), bf16[8,64,1024]{2,1,0:T(8,128)(2,1)S(1)}, u32[]{:S(2)}, u32[]{:S(2)}) %all-to-all-start.1) | async-done | bytes 1048608 | tf_op jit(solution)/shard_map/all_to_all | solution.py:186
  (131 shorter events, 28.4 us)
Async XLA Ops:
  6.5 39.3 %all-gather.19.cloned.1.call-start = ((), (), s32[]{:S(2)}) async-start(), calls=%async_computation.6 | async-start | bytes 2359296 | tf_op jit(solution)/shard_map/all_gather | solution.py:15
  7.3 6.5 %copy-start.2 = (bf16[128,1024]{1,0:T(8,128)(2,1)S(1)}, bf16[128,1024]{1,0:T(8,128)(2,1)}, u32[]{:S(2)}) copy-start(bf16[128,1024]{1,0:T(8,128)(2,1)} %param.22) | copy-start | bytes 786436
  11.2 3.1 copy-start.3
  13.7 80.0 %all-gather.21.cloned.1.call-start = ((), (), s32[]{:S(2)}) async-start(), calls=%async_computation.7 | async-start | bytes 4718592 | tf_op jit(solution)/shard_map/all_gather | solution.py:15
  14.0 3.3 copy-start
  14.8 26.0 %copy-start.6 = (f32[2,512]{1,0:T(2,128)S(1)}, f32[2,512]{1,0:T(2,128)}, u32[]{:S(2)}) copy-start(f32[2,512]{1,0:T(2,128)} %param.26) | copy-start | bytes 12292
  17.1 122.9 %all-gather.11.cloned.1.call-start = ((), (), s32[]{:S(2)}) async-start(), calls=%async_computation.2 | async-start | bytes 1310720 | tf_op jit(solution)/shard_map/all_gather | solution.py:146
  111.8 3.5 copy-start.5
  111.9 111.7 %copy-start.1 = (bf16[128,1024]{1,0:T(8,128)(2,1)S(1)}, bf16[128,1024]{1,0:T(8,128)(2,1)}, u32[]{:S(2)}) copy-start(bf16[128,1024]{1,0:T(8,128)(2,1)} %param.18) | copy-start | bytes 786436
  114.7 108.9 %all-gather.13.cloned.1.call-start = ((), (), s32[]{:S(2)}) async-start(), calls=%async_computation.3 | async-start | bytes 9437184 | tf_op jit(solution)/shard_map/all_gather | solution.py:150
  115.3 203.2 %all-gather.15.cloned.1.call-start = ((), (), s32[]{:S(2)}) async-start(), calls=%async_computation.4 | async-start | bytes 5242880 | tf_op jit(solution)/shard_map/all_gather | solution.py:174
  117.0 121.4 %copy-start.4 = (f32[1024]{0:T(1024)S(1)}, f32[1024]{0:T(1024)}, u32[]{:S(2)}) copy-start(f32[1024]{0:T(1024)} %param.28) | copy-start | bytes 12292
  268.7 94.2 %all-gather.17.cloned.1.call-start = ((), (), s32[]{:S(2)}) async-start(), calls=%async_computation.5 | async-start | bytes 2621440 | tf_op jit(solution)/shard_map/all_gather | solution.py:182
  318.5 5.9 %copy-start.8 = (bf16[1,4096,512]{2,1,0:T(8,128)(2,1)S(1)}, bf16[1,4096,512]{2,1,0:T(8,128)(2,1)}, u32[]{:S(2)}) copy-start(bf16[1,4096,512]{2,1,0:T(8,128)(2,1)} %param.32) | copy-start | bytes 12582916
  318.5 5.9 %copy-start.9 = (bf16[8,64,4096]{2,1,0:T(8,128)(2,1)S(1)}, bf16[8,64,4096]{2,1,0:T(8,128)(2,1)}, u32[]{:S(2)}) copy-start(bf16[8,64,4096]{2,1,0:T(8,128)(2,1)} %all-gather.15.cloned.1.call-done) | copy-start | bytes 12582916
  327.6 45.9 %copy-start.7 = (f32[128,2]{0,1:T(2,128)S(1)}, f32[128,2]{0,1:T(2,128)}, u32[]{:S(2)}) copy-start(f32[128,2]{0,1:T(2,128)} %param.30) | copy-start | bytes 3076
  369.0 31.2 %all-to-all-start.1 = ((bf16[8,64,1024]{2,1,0:T(8,128)(2,1)}), bf16[8,64,1024]{2,1,0:T(8,128)(2,1)S(1)}, u32[]{:S(2)}, u32[]{:S(2)}) async-start(bf16[8,64,1024]{2,1,0:T(8,128)(2,1)} %fusion.10), calls=%async_computation.1 | async-start | bytes 2097152 | tf_op jit(solution)/shard_map/all_to_all | solution.py:186
Sparse Core Ops, SparseCore 0:
  13.9 31.9 all-gather.18
  47.4 46.2 all-gather.20
  114.8 25.1 all-gather.10
  141.5 82.0 all-gather.12
  268.8 49.6 all-gather.14
  327.8 35.0 all-gather.16
where the time goes:
time: 409 us; the launch traced here: 408 us
  waiting for transfers between devices  271 us (66%)
  blocking collectives  62.1 us (15%)
  matrix products  26.3 us (6%)
  other arithmetic  21.3 us (5%)
  between operations  14 us (3%)
  local copies, waits for them, and re-layouts  8.67 us (2%)
  starting transfers between devices  4.99 us (1%)
    all_gather x1, waiting for transfers between devices, per_device(): lax.all_gather(out_weight, 'sp', axis=1, tiled=True)  83.5 us
    all_gather x2, waiting for transfers between devices, entering_2(): everything = jax.tree.map(lambda part: lax.all_gather(part, axis), array)  52.4 us
    all_gather x1, waiting for transfers between devices, per_device(): expert_arrived = lax.all_gather(arrived, 'tp', axis=2, tiled=True)  49.5 us
    all_gather x1, waiting for transfers between devices, per_device(): lax.all_gather(hidden, 'tp', axis=2, tiled=True)  35.2 us
    all_to_all x1, blocking collectives, per_device(): lax.all_to_all(outgoing, 'sp', split_axis=0, concat_axis=0, tiled=True)  29.7 us
    all_to_all x1, waiting for transfers between devices, per_device(): lax.all_to_all(expert_out, 'sp', split_axis=0, concat_axis=0, tiled=True)  26.4 us
    all_gather x1, waiting for transfers between devices, per_device(): gathered = lax.all_gather(stacked, 'tp', axis=2, tiled=True)  23 us
    all_gather x2, blocking collectives, entering_2(): everything = jax.tree.map(lambda part: lax.all_gather(part, axis), array)  22.6 us
  transfers between devices with their start and end apart: 7, of which 7 were waited for; matrix products, arithmetic and copies ran while one was open for 2% of the time, Pallas kernels for 0%

commit v1 on v0

--- a/solution.py
+++ b/solution.py
@@ -1,30 +1,407 @@
 import jax
 import jax.numpy as jnp
 from jax import lax
+from jax.experimental import pallas as pl
+from jax.experimental.pallas import tpu as pltpu
 from jax.sharding import PartitionSpec as P
 
-D = 4096
+MESH = pl.DeviceIdType.MESH
 
 
 EPS = 1e-06
 THETA = 10000.0
 
 
-def entering_2(array, axis, combine, identity):
-    devices, place = (lax.axis_size(axis), lax.axis_index(axis))
-    everything = jax.tree.map(lambda part: lax.all_gather(part, axis), array)
-    start = jax.tree.map(
-        lambda part, zero: jnp.broadcast_to(jnp.asarray(zero, part.dtype), part.shape),
-        array,
-        identity,
-    )
-
-    def step(k, before):
-        reached = k < place
-        new = combine(before, jax.tree.map(lambda part: part[k], everything))
-        return jax.tree.map(lambda a, b: jnp.where(reached, a, b), new, before)
-
-    return lax.fori_loop(0, devices, step, start)
+def greet(axes):
+    barrier = pltpu.get_barrier_semaphore()
+    total = 0
+    for axis in axes:
+        count, me = lax.axis_size(axis), lax.axis_index(axis)
+
+        def signal(k, _, axis=axis, count=count, me=me):
+            pl.semaphore_signal(
+                barrier, inc=1, device_id={axis: (me + k) % count}, device_id_type=MESH
+            )
+            return 0
+
+        lax.fori_loop(1, count, signal, 0)
+        total += count - 1
+    pl.semaphore_wait(barrier, total)
+
+
+def remote(source, target, send_sem, recv_sem, axis, index):
+    return pltpu.make_async_remote_copy(
+        src_ref=source,
+        dst_ref=target,
+        send_sem=send_sem,
+        recv_sem=recv_sem,
+        device_id={axis: index},
+        device_id_type=MESH,
+    )
+
+
+def chain_kernel(update_ref, fall_ref, out_ref, held, outgoing, send_sem, recv_sem):
+    count, me = lax.axis_size("sp"), lax.axis_index("sp")
+    pieces = update_ref.shape[0]
+    right, left = (me + 1) % count, (me + count - 1) % count
+    barrier = pltpu.get_barrier_semaphore()
+    for neighbour in (left, right):
+        pl.semaphore_signal(barrier, inc=1, device_id={"sp": neighbour}, device_id_type=MESH)
+    pl.semaphore_wait(barrier, 2)
+
+    def hop(c):
+        return remote(
+            outgoing.at[c], held.at[c], send_sem.at[c], recv_sem.at[c], "sp", right
+        )
+
+    def step(c, _):
+        @pl.when(me == 0)
+        def _():
+            held[c] = jnp.zeros(held.shape[1:], held.dtype)
+
+        @pl.when(me > 0)
+        def _():
+            hop(c).wait_recv()
+
+        @pl.when(me < count - 1)
+        def _():
+            outgoing[c] = (fall_ref[c] * held[c].astype(jnp.float32) + update_ref[c]).astype(
+                outgoing.dtype
+            )
+            hop(c).start()
+
+        out_ref[c] = held[c]
+        return 0
+
+    lax.fori_loop(0, pieces, step, 0)
+
+    @pl.when(me < count - 1)
+    def _():
+        def finish(c, _):
+            hop(c).wait_send()
+            return 0
+
+        lax.fori_loop(0, pieces, finish, 0)
+
+
+def entering_states(update, fall):
+    pieces, rows, columns = update.shape
+    return pl.pallas_call(
+        chain_kernel,
+        out_shape=jax.ShapeDtypeStruct(update.shape, jnp.bfloat16),
+        in_specs=[pl.BlockSpec(memory_space=pltpu.VMEM)] * 2,
+        out_specs=pl.BlockSpec(memory_space=pltpu.VMEM),
+        scratch_shapes=[
+            pltpu.VMEM((pieces, rows, columns), jnp.bfloat16),
+            pltpu.VMEM((pieces, rows, columns), jnp.bfloat16),
+            pltpu.SemaphoreType.DMA((pieces,)),
+            pltpu.SemaphoreType.DMA((pieces,)),
+        ],
+        compiler_params=pltpu.CompilerParams(collective_id=0, has_side_effects=True),
+    )(update, fall)
+
+
+def gather_kernel(part_ref, out_ref, held, send_sem, recv_sem):
+    count, me = lax.axis_size("tp"), lax.axis_index("tp")
+    width = part_ref.shape[2]
+    greet(("tp",))
+
+    def place(index):
+        return held.at[:, :, pl.ds(pl.multiple_of(index * width, width), width)]
+
+    def start(k, _):
+        remote(part_ref, place(me), send_sem.at[k], recv_sem.at[me], "tp", (me + k) % count).start()
+        return 0
+
+    lax.fori_loop(1, count, start, 0)
+    held[:, :, pl.ds(pl.multiple_of(me * width, width), width)] = part_ref[...]
+
+    def finish(k, _):
+        other = (me + k) % count
+        remote(part_ref, place(other), send_sem.at[k], recv_sem.at[other], "tp", other).wait()
+        return 0
+
+    lax.fori_loop(1, count, finish, 0)
+    out_ref[...] = held[...]
+
+
+def gather_heads(part, count):
+    whole = part.shape[:2] + (part.shape[2] * count,)
+    return pl.pallas_call(
+        gather_kernel,
+        out_shape=jax.ShapeDtypeStruct(whole, part.dtype),
+        in_specs=[pl.BlockSpec(memory_space=pltpu.VMEM)],
+        out_specs=pl.BlockSpec(memory_space=pltpu.VMEM),
+        scratch_shapes=[
+            pltpu.VMEM(whole, part.dtype),
+            pltpu.SemaphoreType.DMA((count,)),
+            pltpu.SemaphoreType.DMA((count,)),
+        ],
+        compiler_params=pltpu.CompilerParams(collective_id=1, has_side_effects=True),
+    )(part)
+
+
+def experts_kernel(
+    stream_ref,
+    gain_ref,
+    select_ref,
+    gate_hbm,
+    up_hbm,
+    down_hbm,
+    out_ref,
+    w_gate,
+    w_up,
+    w_down,
+    squares,
+    outgoing,
+    arrived,
+    hidden,
+    result,
+    returned,
+    acc_a,
+    acc_b,
+    acc_c,
+    load_sem,
+    sq_send,
+    sq_recv,
+    disp_send,
+    disp_recv,
+    fwd_send,
+    fwd_recv,
+    hid_send,
+    hid_recv,
+    ret_send,
+    ret_recv,
+):
+    n_sp, n_tp = lax.axis_size("sp"), lax.axis_size("tp")
+    s, t = lax.axis_index("sp"), lax.axis_index("tp")
+    half = n_sp // 2
+    cap = outgoing.shape[0] // n_sp
+    cols = stream_ref.shape[1]
+    units = w_gate.shape[1]
+    loads = [
+        pltpu.make_async_copy(source.at[0], target, load_sem.at[i])
+        for i, (source, target) in enumerate(
+            ((gate_hbm, w_gate), (up_hbm, w_up), (down_hbm, w_down))
+        )
+    ]
+    for load in loads:
+        load.start()
+    greet(("sp", "tp"))
+
+    def rows_of(p):
+        return pl.ds(pl.multiple_of(p * cap, cap), cap)
+
+    def group_base(g):
+        return ((s // half + g) % 2) * half
+
+    def group_rows(g):
+        return pl.ds(pl.multiple_of(group_base(g) * cap, half * cap), half * cap)
+
+    stream = stream_ref[...]
+    own = jnp.sum(stream * stream, axis=1, keepdims=True)
+    squares[t] = jnp.broadcast_to(own, squares.shape[1:])
+
+    def square_copy(k, source):
+        block, other = squares.at[source], (t + k) % n_tp
+        return remote(block, block, sq_send.at[k], sq_recv.at[source], "tp", other)
+
+    def square_start(k, _):
+        square_copy(k, t).start()
+        return 0
+
+    def square_wait(k, _):
+        square_copy(k, (t + k) % n_tp).wait()
+        return 0
+
+    lax.fori_loop(1, n_tp, square_start, 0)
+    lax.fori_loop(1, n_tp, square_wait, 0)
+    total = squares[0]
+    for p in range(1, n_tp):
+        total = total + squares[p]
+    scale = lax.rsqrt(total[:, 0:1] / (cols * n_tp) + EPS)
+    normed = (stream_ref[...] * scale * gain_ref[...]).astype(jnp.bfloat16)
+    outgoing[...] = jnp.dot(
+        select_ref[...], normed, preferred_element_type=jnp.float32
+    ).astype(jnp.bfloat16)
+
+    def dispatch(p, q):
+        return remote(
+            outgoing.at[rows_of(p)],
+            arrived.at[t, rows_of(q)],
+            disp_send.at[p],
+            disp_recv.at[q],
+            "sp",
+            p,
+        )
+
+    def others(g, action):
+        def body(j, _):
+            p = group_base(g) + (s + j) % half
+
+            @pl.when(p != s)
+            def _():
+                action(p)
+
+            return 0
+
+        lax.fori_loop(0, half, body, 0)
+
+    for g in range(2):
+        others(g, lambda p: dispatch(p, s).start())
+    arrived[t, rows_of(s)] = outgoing[rows_of(s)]
+
+    def forward(g):
+        def body(j, _):
+            p = group_base(g) + (s + j) % half
+
+            @pl.when(p != s)
+            def _():
+                dispatch(p, p).wait_recv()
+
+            def send(k, _):
+                block = arrived.at[t, rows_of(p)]
+                remote(
+                    block, block, fwd_send.at[g, k], fwd_recv.at[g, t], "tp", (t + k) % n_tp
+                ).start()
+                return 0
+
+            lax.fori_loop(1, n_tp, send, 0)
+            return 0
+
+        lax.fori_loop(0, half, body, 0)
+
+    def forwarded(g, k):
+        other = (t + k) % n_tp
+        block = arrived.at[other, group_rows(g)]
+        return remote(block, block, fwd_send.at[g, k], fwd_recv.at[g, other], "tp", other)
+
+    def hidden_copy(g, k, source):
+        block = hidden.at[source, group_rows(g)]
+        return remote(
+            block, block, hid_send.at[g, k], hid_recv.at[g, source], "tp", (t + k) % n_tp
+        )
+
+    for g in range(2):
+        forward(g)
+    for load in loads:
+        load.wait()
+
+    def through_units(g):
+        acc_a[...] = jnp.zeros_like(acc_a)
+        acc_b[...] = jnp.zeros_like(acc_b)
+
+        def body(k, _):
+            @pl.when(k > 0)
+            def _():
+                forwarded(g, k).wait_recv()
+
+            p = (t + k) % n_tp
+            part = pl.ds(pl.multiple_of(p * cols, cols), cols)
+            rows = arrived[p, group_rows(g)]
+            acc_a[...] += jnp.dot(rows, w_gate[part, :], preferred_element_type=jnp.float32)
+            acc_b[...] += jnp.dot(rows, w_up[part, :], preferred_element_type=jnp.float32)
+            return 0
+
+        lax.fori_loop(0, n_tp, body, 0)
+        hidden[t, group_rows(g)] = (jax.nn.silu(acc_a[...]) * acc_b[...]).astype(jnp.bfloat16)
+
+        def send(k, _):
+            hidden_copy(g, k, t).start()
+            return 0
+
+        lax.fori_loop(1, n_tp, send, 0)
+
+    def give_back(p, q):
+        return remote(
+            result.at[rows_of(p)], returned.at[rows_of(q)], ret_send.at[p], ret_recv.at[q], "sp", p
+        )
+
+    def through_down(g):
+        acc_c[...] = jnp.zeros_like(acc_c)
+
+        def body(k, _):
+            p = (t + k) % n_tp
+
+            @pl.when(k > 0)
+            def _():
+                hidden_copy(g, k, p).wait_recv()
+
+            part = pl.ds(pl.multiple_of(p * units, units), units)
+            acc_c[...] += jnp.dot(
+                hidden[p, group_rows(g)], w_down[part, :], preferred_element_type=jnp.float32
+            )
+            return 0
+
+        lax.fori_loop(0, n_tp, body, 0)
+        result[group_rows(g)] = acc_c[...].astype(jnp.bfloat16)
+        others(g, lambda p: give_back(p, s).start())
+
+    for g in ORDER:
+        through_units(g)
+    for g in ORDER:
+        through_down(g)
+    returned[rows_of(s)] = result[rows_of(s)]
+    for g in range(2):
+        others(g, lambda p: give_back(p, p).wait_recv())
+    out_ref[...] = returned[...]
+    for g in range(2):
+        others(g, lambda p: dispatch(p, s).wait_send())
+        others(g, lambda p: give_back(p, s).wait_send())
+
+        def finish(k, _, g=g):
+            forwarded(g, k).wait_send()
+            hidden_copy(g, k, t).wait_send()
+            return 0
+
+        lax.fori_loop(1, n_tp, finish, 0)
+
+
+ORDER = (0, 1)
+
+
+def through_experts(stream, gain, select, w_gate, w_up, w_down, n_sp, n_tp):
+    count, cols = stream.shape
+    slots = select.shape[0]
+    width, units = w_gate.shape[1:]
+    bf16, f32 = jnp.bfloat16, jnp.float32
+    dma = pltpu.SemaphoreType.DMA
+    vmem = pl.BlockSpec(memory_space=pltpu.VMEM)
+    hbm = pl.BlockSpec(memory_space=pl.ANY)
+    return pl.pallas_call(
+        experts_kernel,
+        out_shape=jax.ShapeDtypeStruct((slots, cols), bf16),
+        in_specs=[vmem] * 3 + [hbm] * 3,
+        out_specs=vmem,
+        scratch_shapes=[
+            pltpu.VMEM((width, units), bf16),
+            pltpu.VMEM((width, units), bf16),
+            pltpu.VMEM(w_down.shape[1:], bf16),
+            pltpu.VMEM((n_tp, count, 128), f32),
+            pltpu.VMEM((slots, cols), bf16),
+            pltpu.VMEM((n_tp, slots, cols), bf16),
+            pltpu.VMEM((n_tp, slots, units), bf16),
+            pltpu.VMEM((slots, cols), bf16),
+            pltpu.VMEM((slots, cols), bf16),
+            pltpu.VMEM((slots // 2, units), f32),
+            pltpu.VMEM((slots // 2, units), f32),
+            pltpu.VMEM((slots // 2, cols), f32),
+            dma((3,)),
+            dma((n_tp,)),
+            dma((n_tp,)),
+            dma((n_sp,)),
+            dma((n_sp,)),
+            dma((2, n_tp)),
+            dma((2, n_tp)),
+            dma((2, n_tp)),
+            dma((2, n_tp)),
+            dma((n_sp,)),
+            dma((n_sp,)),
+        ],
+        compiler_params=pltpu.CompilerParams(
+            collective_id=2, has_side_effects=True, vmem_limit_bytes=50 * 2**20
+        ),
+    )(stream, gain, select, w_gate, w_up, w_down)
 
 
 def rotate(block, positions):
@@ -64,9 +441,9 @@
     cross_part = (
         jnp.einsum(
             "ihd,hdv->ihv",
-            rot_queries.astype(jnp.float32),
+            rot_queries,
             state_in,
-            precision=lax.Precision.HIGHEST,
+            preferred_element_type=jnp.float32,
         )
         * jnp.exp(decay_sum)[:, :, None]
     )
@@ -125,36 +502,25 @@
     within_a, decay_sum_a, fall_a, update_a = block_terms(query_a, key_a, value_a, log_decay[:, 0])
     within_b, decay_sum_b, fall_b, update_b = block_terms(query_b, key_b, value_b, log_decay[:, 1])
 
-    def combine(before_part, after_part):
-        return (
-            before_part[0] * after_part[0],
-            after_part[0][:, None, None] * before_part[1] + after_part[1],
-            before_part[2] * after_part[2],
-            after_part[2][:, None, None] * before_part[3] + after_part[3],
-        )
-
-    identity = (
-        jnp.ones_like(fall_a),
-        jnp.zeros_like(update_a),
-        jnp.ones_like(fall_b),
-        jnp.zeros_like(update_b),
-    )
-    entering = entering_2((fall_a, update_a, fall_b, update_b), "sp", combine, identity)
-    output_a = final_result(query_a, decay_sum_a, within_a, entering[1], gates[:, 0], head_gain[0])
-    output_b = final_result(query_b, decay_sum_b, within_b, entering[3], gates[:, 1], head_gain[1])
-    stacked = jnp.stack([output_a, output_b], axis=1)
-    gathered = lax.all_gather(stacked, "tp", axis=2, tiled=True)
-    mixed = jnp.einsum(
-        "tgk,gkd->td",
-        gathered,
-        lax.all_gather(out_weight, "sp", axis=1, tiled=True),
-        preferred_element_type=jnp.float32,
+    n_sp, n_tp = lax.axis_size("sp"), lax.axis_size("tp")
+    value_size = update_a.shape[2]
+    piece = update_a.shape[1]
+    parts = update_b.shape[1] // piece
+    update = jnp.concatenate([update_a, update_b.reshape(-1, piece, value_size)], axis=0)
+    fall = jnp.concatenate([fall_a, jnp.repeat(fall_b, parts)])
+    fall = jnp.broadcast_to(fall[:, None, None], (fall.shape[0], 1, value_size))
+    entering = entering_states(update, fall)
+    state_a = entering[:head_count]
+    state_b = entering[head_count:].reshape(update_b.shape)
+    output_a = final_result(query_a, decay_sum_a, within_a, state_a, gates[:, 0], head_gain[0])
+    output_b = final_result(query_b, decay_sum_b, within_b, state_b, gates[:, 1], head_gain[1])
+    gathered = gather_heads(jnp.stack([output_a, output_b], axis=0), n_tp)
+    weight = lax.all_gather(out_weight, "sp", axis=1, tiled=True)
+    mixed = (
+        jnp.dot(gathered[0], weight[0], preferred_element_type=jnp.float32)
+        + jnp.dot(gathered[1], weight[1], preferred_element_type=jnp.float32)
     ).astype(jnp.bfloat16)
     stream = residual.astype(jnp.float32) + mixed.astype(jnp.float32)
-    square_sum = lax.psum(jnp.sum(stream * stream, axis=1), "tp")
-    normed = (stream * lax.rsqrt(square_sum / D + EPS)[:, None] * norm_gain[None, :]).astype(
-        jnp.bfloat16
-    )
     experts = lax.axis_size("sp")
     capacity = 4 * row_count // experts
     one_hot = (routes[:, :, None] == jnp.arange(experts, dtype=jnp.int32)[None, None, :]).astype(
@@ -167,24 +533,8 @@
     slot_ids = jnp.arange(experts * capacity, dtype=jnp.int32)
     choose = target[:, :, None] == slot_ids[None, None, :]
     select = jnp.sum(choose.astype(jnp.int32), axis=1).astype(jnp.bfloat16).T
-    w_gate, w_up, w_down = (expert_gate[0], expert_up[0], expert_down[0])
-    outgoing = jnp.dot(select, normed, preferred_element_type=jnp.float32).astype(jnp.bfloat16)
-    outgoing = outgoing.reshape(experts, capacity, normed.shape[1])
-    arrived = lax.all_to_all(outgoing, "sp", split_axis=0, concat_axis=0, tiled=True)
-    expert_arrived = lax.all_gather(arrived, "tp", axis=2, tiled=True)
-    gate_part = jnp.einsum(
-        "sck,kf->scf", expert_arrived, w_gate, preferred_element_type=jnp.float32
-    )
-    up_part = jnp.einsum("sck,kf->scf", expert_arrived, w_up, preferred_element_type=jnp.float32)
-    hidden = (jax.nn.silu(gate_part) * up_part).astype(jnp.bfloat16)
-    expert_out = jnp.einsum(
-        "scf,fd->scd",
-        lax.all_gather(hidden, "tp", axis=2, tiled=True),
-        w_down,
-        preferred_element_type=jnp.float32,
-    ).astype(jnp.bfloat16)
-    returned = lax.all_to_all(expert_out, "sp", split_axis=0, concat_axis=0, tiled=True).reshape(
-        experts * capacity, -1
+    returned = through_experts(
+        stream, norm_gain[None, :], select, expert_gate, expert_up, expert_down, n_sp, n_tp
     )
     first_pick = jnp.dot(
         choose[:, 0].astype(jnp.bfloat16), returned, preferred_element_type=jnp.float32

time: 409 us -> 213 us (0.52)
  waiting for transfers between devices: 271 us -> 47.6 us
  Pallas kernels: 0 us -> 125 us
  blocking collectives: 62.1 us -> 0 us
  other arithmetic: 21.3 us -> 5.92 us
  matrix products: 26.3 us -> 11.1 us
  starting transfers between devices: 4.99 us -> 0.01 us
    all_gather x6 -> x1, waiting for transfers between devices: 244 us -> 46.9 us  [per_device(): weight = lax.all_gather(out_weight, 'sp', axis=1, tiled=True)]
    pallas_call x0 -> x3, Pallas kernels: none -> 125 us  [the longest x1 105 us: through_experts(): pl.pallas_call(experts_kernel, out_shape=jax.ShapeDtypeStruct((slots, col...]
    all_to_all x1 -> x0, blocking collectives: 29.7 us -> none  [per_device(): lax.all_to_all(outgoing, 'sp', split_axis=0, concat_axis=0, tiled=True)]
    all_to_all x1 -> x0, waiting for transfers between devices: 26.4 us -> none  [per_device(): lax.all_to_all(expert_out, 'sp', split_axis=0, concat_axis=0, tiled=True)]
    all_gather x2 -> x0, blocking collectives: 22.6 us -> none  [entering_2(): everything = jax.tree.map(lambda part: lax.all_gather(part, axis), array)]
    select_n x16 -> x0, other arithmetic: 17.8 us -> none  [step(): return jax.tree.map(lambda a, b: jnp.where(reached, a, b), new, before)]
    dot_general x7 -> x4, matrix products: 21.9 us -> 7.53 us  [the longest x1 3.06 us: per_device(): jnp.dot(gathered[1], weight[1], preferred_element_type=jnp.float32)]
    psum x1 -> x0, blocking collectives: 9.84 us -> none  [per_device(): square_sum = lax.psum(jnp.sum(stream * stream, axis=1), 'tp')]
  transfers between devices with their start and end apart: 7 -> 1, of which waited for: 7 -> 1; matrix products, arithmetic and copies ran while one was open for 2% -> 9% of each run, Pallas kernels for 0% -> 10%
where the time goes in v1:
time: 213 us
  Pallas kernels  125 us (59%)
  waiting for transfers between devices  47.6 us (22%)
  between operations  13.9 us (7%)
  matrix products  11.1 us (5%)
  local copies, waits for them, and re-layouts  9.01 us (4%)
  other arithmetic  5.92 us (3%)
    pallas_call x1, Pallas kernels, through_experts(): pl.pallas_call(experts_kernel, out_shape=jax.ShapeDtypeStruct((slots, col...  105 us
    all_gather x1, waiting for transfers between devices, per_device(): weight = lax.all_gather(out_weight, 'sp', axis=1, tiled=True)  46.9 us
    pallas_call x1, Pallas kernels, gather_heads(): pl.pallas_call(gather_kernel, out_shape=jax.ShapeDtypeStruct(whole, part....  12.4 us
    pallas_call x1, Pallas kernels, entering_states(): pl.pallas_call(chain_kernel, out_shape=jax.ShapeDtypeStruct(update.shape,...  8.07 us
    unnamed x40, local copies, waits for them, and re-layouts  4.55 us
  transfers between devices with their start and end apart: 1, of which 1 were waited for; matrix products, arithmetic and copies ran while one was open for 9% of the time, Pallas kernels for 10%

profile of v1, /device:TPU:0, one launch (start us, length us, event | category | flops | bytes accessed | tf_op | source)
XLA Modules:
  0.0 213.0 jit_solution(3680007109765119164)
XLA Ops:
  6.5 0.7 all-gather.2.cloned.1.call-update
  7.3 0.8 copy.156
  8.3 1.1 copy.131
  9.8 1.1 copy.145
  11.6 0.7 fusion.70
  12.3 0.4 fusion.64
  14.5 0.6 copy.125
  15.2 0.4 fusion.63
  17.1 0.8 multiply_subtract_fusion
  17.9 0.4 fusion.20
  18.3 1.0 pad_maximum_fusion.update_ref
  19.3 0.7 broadcast_in_dim.39.fall_ref
  20.0 8.1 %shard_map.154 = bf16[12,128,128]{2,1,0:T(8,128)(2,1)} custom-call(f32[12,128,128]{2,1,0:T(8,128)} %pad_maximum_fusion.update_ref, f32[12,1,128]{2,1,0:T(1,128)} %broadcast_in_dim.39.fall_ref), custom_call_target="tpu_custom_call" | custom-call | tf_op jit(solution)/shard_map/pallas_call | solution.py:89
  28.1 1.1 convolution_bitcast_fusion.3
  29.3 1.2 multiply_reduce_fusion.1
  31.1 0.4 convolution_bitcast_fusion.2
  32.1 0.7 pad_maximum_fusion.2.part_ref
  32.8 12.4 %shard_map.155 = bf16[2,128,2048]{2,1,0:T(8,128)(2,1)} custom-call(bf16[2,128,512]{2,1,0:T(8,128)(2,1)} %pad_maximum_fusion.2.part_ref), custom_call_target="tpu_custom_call" | custom-call | tf_op jit(solution)/shard_map/pallas_call | solution.py:130
  45.2 0.6 reduce-window.6
  46.8 46.9 %all-gather.2.cloned.1.call-done = bf16[2,2048,1024]{2,1,0:T(8,128)(2,1)} async-done(((bf16[2,256,1024]{2,1,0:T(8,128)(2,1)}), bf16[2,2048,1024]{2,1,0:T(8,128)(2,1)}) %all-gather.2.cloned.1.call-update) | async-done | bytes 8388624 | tf_op jit(solution)/shard_map/all_gather | solution.py:518
  93.7 3.1 %fusion = f32[128,1024]{1,0:T(8,128)S(1)} fusion(bf16[2,2048,1024]{2,1,0:T(8,128)(2,1)} %all-gather.2.cloned.1.call-done, bf16[2,128,2048]{2,1,0:T(8,128)(2,1)} %shard_map.155), kind=kOutput, calls=%fused_computation.1 | convolution fusion | flops 536870912 | bytes 5242880 | tf_op jit(solution)/shard_map/dot_general | solution.py:521
  96.8 3.0 %fusion.7.stream_ref = f32[128,1024]{1,0:T(8,128)S(1)} fusion(f32[128,1024]{1,0:T(8,128)S(1)} %fusion, bf16[2,2048,1024]{2,1,0:T(8,128)(2,1)} %all-gather.2.cloned.1.call-done, bf16[2,128,2048]{2,1,0:T(8,128)(2,1)S(1)} %copy-done.1, bf16[128,1024]{1,0:T(8,128)(2,1)S(1)} %copy-done.12), kind=kOutput, calls=%fused_computation.11 | convolution fusion | flops 537526272 | bytes 6029312 | tf_op jit(solution)/shard_map/dot_general | solution.py:520
  99.8 104.9 %shard_map.156 = bf16[512,1024]{1,0:T(8,128)(2,1)S(1)} custom-call(f32[128,1024]{1,0:T(8,128)S(1)} %fusion.7.stream_ref, f32[1,1024]{1,0:T(1,128)S(1)} %bitcast.98, bf16[512,128]{1,0:T(8,128)(2,1)S(1)} %convert_bitcast_fusion.select_ref, bf16[1,4096,512]{2,1,0:T(8,128)(2,1)} %gate_hbm.1, bf16[1,4096,512]{2,1,0:T(8,128)(2,1)} %up_hbm.1, ...), custom_call_target="tpu_custom_call" | custom-call | tf_op jit(solution)/shard_map/pallas_call | solution.py:371
  205.1 1.0 fusion.8
  (99 shorter events, 7.0 us)
Async XLA Ops:
  6.5 4.7 %copy-start.9 = (f32[128,2,4]{0,2,1:T(4,128)S(1)}, f32[128,2,4]{0,2,1:T(4,128)}, u32[]{:S(2)}) copy-start(f32[128,2,4]{0,2,1:T(4,128)} %param.23) | copy-start | bytes 12292
  6.5 5.8 %copy-start.2 = (bf16[128,2,512]{2,1,0:T(2,128)(2,1)S(1)}, bf16[128,2,512]{2,1,0:T(2,128)(2,1)}, u32[]{:S(2)}) copy-start(bf16[128,2,512]{2,1,0:T(2,128)(2,1)} %param.21) | copy-start | bytes 786436
  6.5 6.3 %copy-start.6 = (bf16[128,512]{1,0:T(8,128)(2,1)S(1)}, bf16[128,512]{1,0:T(8,128)(2,1)}, u32[]{:S(2)}) copy-start(bf16[128,512]{1,0:T(8,128)(2,1)} %param.17) | copy-start | bytes 393220
  6.5 87.2 %all-gather.2.cloned.1.call-start = ((), (), s32[]{:S(2)}) async-start(), calls=%async_computation | async-start | bytes 9437184 | tf_op jit(solution)/shard_map/all_gather | solution.py:518
  9.5 3.8 %copy-start.7 = (bf16[128,512]{1,0:T(8,128)(2,1)S(1)}, bf16[128,512]{1,0:T(8,128)(2,1)}, u32[]{:S(2)}) copy-start(bf16[128,512]{1,0:T(8,128)(2,1)} %param.18) | copy-start | bytes 393220
  10.9 4.3 %copy-start.3 = (bf16[128,2,512]{2,1,0:T(2,128)(2,1)S(1)}, bf16[128,2,512]{2,1,0:T(2,128)(2,1)}, u32[]{:S(2)}) copy-start(bf16[128,2,512]{2,1,0:T(2,128)(2,1)} %param.22) | copy-start | bytes 786436
  17.9 12.6 %copy-start.10 = (f32[2,512]{1,0:T(2,128)S(1)}, f32[2,512]{1,0:T(2,128)}, u32[]{:S(2)}) copy-start(f32[2,512]{1,0:T(2,128)} %param.24) | copy-start | bytes 12292
  17.9 12.9 %copy-start.5 = (f32[128,4]{1,0:T(8,128)S(1)}, f32[128,4]{1,0:T(8,128)}, u32[]{:S(2)}) copy-start(f32[128,4]{1,0:T(8,128)} %get-tuple-element.31) | copy-start | bytes 6148
  17.9 13.2 %copy-start.4 = (bf16[128,4,128]{2,0,1:T(8,128)(2,1)S(1)}, bf16[128,4,128]{2,0,1:T(8,128)(2,1)}, u32[]{:S(2)}) copy-start(bf16[128,4,128]{2,0,1:T(8,128)(2,1)} %get-tuple-element.28) | copy-start | bytes 393220
  28.1 3.4 %slice-start = ((bf16[12,128,128]{2,1,0:T(8,128)(2,1)}), bf16[8,128,128]{2,1,0:T(8,128)(2,1)S(1)}, s32[]{:S(2)}) async-start(bf16[12,128,128]{2,1,0:T(8,128)(2,1)} %shard_map.154), calls=%async_computation.1 | async-start | bytes 524288 | tf_op jit(solution)/shard_map/slice | solution.py:514
  29.3 17.1 %copy-start.8 = (s32[128,2]{0,1:T(2,128)S(1)}, s32[128,2]{0,1:T(2,128)}, u32[]{:S(2)}) copy-start(s32[128,2]{0,1:T(2,128)} %param.27) | copy-start | bytes 3076
  30.5 16.1 %copy-start.11 = (f32[128,2]{0,1:T(2,128)S(1)}, f32[128,2]{0,1:T(2,128)}, u32[]{:S(2)}) copy-start(f32[128,2]{0,1:T(2,128)} %param.28) | copy-start | bytes 3076
  45.2 51.6 %copy-start.1 = (bf16[2,128,2048]{2,1,0:T(8,128)(2,1)S(1)}, bf16[2,128,2048]{2,1,0:T(8,128)(2,1)}, u32[]{:S(2)}) copy-start(bf16[2,128,2048]{2,1,0:T(8,128)(2,1)} %shard_map.155) | copy-start | bytes 3145732
  45.2 51.6 %copy-start.12 = (bf16[128,1024]{1,0:T(8,128)(2,1)S(1)}, bf16[128,1024]{1,0:T(8,128)(2,1)}, u32[]{:S(2)}) copy-start(bf16[128,1024]{1,0:T(8,128)(2,1)} %param.16) | copy-start | bytes 786436
  96.8 3.0 %copy-start = (f32[1024]{0:T(1024)S(1)}, f32[1024]{0:T(1024)}, u32[]{:S(2)}) copy-start(f32[1024]{0:T(1024)} %param.26) | copy-start | bytes 12292
Sparse Core Ops, SparseCore 0:
  8.9 84.7 all-gather.1

commit v2 on v1

--- a/solution.py
+++ b/solution.py
@@ -168,14 +168,20 @@
     disp_recv,
     fwd_send,
     fwd_recv,
+    fwd_relay_send,
+    fwd_relay_recv,
     hid_send,
     hid_recv,
+    hid_relay_send,
+    hid_relay_recv,
     ret_send,
     ret_recv,
 ):
     n_sp, n_tp = lax.axis_size("sp"), lax.axis_size("tp")
     s, t = lax.axis_index("sp"), lax.axis_index("tp")
-    half = n_sp // 2
+    per_group = n_sp // GROUPS
+    across, down = grid_of(n_tp)
+    x, y = t % across, t // across
     cap = outgoing.shape[0] // n_sp
     cols = stream_ref.shape[1]
     units = w_gate.shape[1]
@@ -193,10 +199,20 @@
         return pl.ds(pl.multiple_of(p * cap, cap), cap)
 
     def group_base(g):
-        return ((s // half + g) % 2) * half
-
-    def group_rows(g):
-        return pl.ds(pl.multiple_of(group_base(g) * cap, half * cap), half * cap)
+        return ((s // per_group + g) % GROUPS) * per_group
+
+    def group_rows(g, part=None):
+        size = per_group * cap
+        start = pl.multiple_of(group_base(g) * cap, size)
+        if part is None:
+            return pl.ds(start, size)
+        return pl.ds(pl.multiple_of(start + part * (size // 2), size // 2), size // 2)
+
+    lines = (
+        [y * across + (x + k) % across for k in range(1, across)],
+        [((y + k) % down) * across + x for k in range(1, down)],
+    )
+    direct = lines[0] + lines[1]
 
     stream = stream_ref[...]
     own = jnp.sum(stream * stream, axis=1, keepdims=True)
@@ -235,68 +251,83 @@
             p,
         )
 
+    def members(g, action):
+        def body(j, _):
+            action(group_base(g) + (s + j) % per_group)
+            return 0
+
+        lax.fori_loop(0, per_group, body, 0)
+
     def others(g, action):
-        def body(j, _):
-            p = group_base(g) + (s + j) % half
-
+        def guarded(p):
             @pl.when(p != s)
             def _():
                 action(p)
 
-            return 0
-
-        lax.fori_loop(0, half, body, 0)
-
-    for g in range(2):
+        members(g, guarded)
+
+    for g in range(GROUPS):
         others(g, lambda p: dispatch(p, s).start())
     arrived[t, rows_of(s)] = outgoing[rows_of(s)]
 
+    def straight(buffer, sems, g, i, source, rows):
+        block = buffer.at[source, rows]
+        return remote(block, block, sems[0].at[g, i], sems[1].at[g, source], "tp", direct[i])
+
+    def relayed(buffer, sems, g, part, i, source, target):
+        block = buffer.at[source, group_rows(g, part)]
+        return remote(
+            block, block, sems[2].at[g, part, i], sems[3].at[g, source, part], "tp", target
+        )
+
+    def relay(buffer, sems, g):
+        for part in range(2):
+            for k, source in enumerate(lines[part]):
+                i = k if part == 0 else len(lines[0]) + k
+                straight(buffer, sems, g, i, source, group_rows(g)).wait_recv()
+                for j, target in enumerate(lines[1 - part]):
+                    relayed(
+                        buffer, sems, g, part, k * len(lines[1 - part]) + j, source, target
+                    ).start()
+
+    def place_of(k):
+        return ((y + k // across) % down) * across + (x + k % across) % across
+
+    def wait_relayed(buffer, sems, g, k):
+        @pl.when((k // across) * (k % across) > 0)
+        def _():
+            source = place_of(k)
+            for part in range(2):
+                relayed(buffer, sems, g, part, 0, source, source).wait_recv()
+
+    def finish_sends(buffer, sems, g):
+        for i in range(len(direct)):
+            straight(buffer, sems, g, i, t, group_rows(g)).wait_send()
+        for part in range(2):
+            for i in range(len(lines[0]) * len(lines[1])):
+                relayed(buffer, sems, g, part, i, t, direct[0]).wait_send()
+
+    arrived_sems = (fwd_send, fwd_recv, fwd_relay_send, fwd_relay_recv)
+    hidden_sems = (hid_send, hid_recv, hid_relay_send, hid_relay_recv)
+
     def forward(g):
-        def body(j, _):
-            p = group_base(g) + (s + j) % half
-
+        def block(p):
             @pl.when(p != s)
             def _():
                 dispatch(p, p).wait_recv()
 
-            def send(k, _):
-                block = arrived.at[t, rows_of(p)]
-                remote(
-                    block, block, fwd_send.at[g, k], fwd_recv.at[g, t], "tp", (t + k) % n_tp
-                ).start()
-                return 0
-
-            lax.fori_loop(1, n_tp, send, 0)
-            return 0
-
-        lax.fori_loop(0, half, body, 0)
-
-    def forwarded(g, k):
-        other = (t + k) % n_tp
-        block = arrived.at[other, group_rows(g)]
-        return remote(block, block, fwd_send.at[g, k], fwd_recv.at[g, other], "tp", other)
-
-    def hidden_copy(g, k, source):
-        block = hidden.at[source, group_rows(g)]
-        return remote(
-            block, block, hid_send.at[g, k], hid_recv.at[g, source], "tp", (t + k) % n_tp
-        )
-
-    for g in range(2):
-        forward(g)
-    for load in loads:
-        load.wait()
+            for i in range(len(direct)):
+                straight(arrived, arrived_sems, g, i, t, rows_of(p)).start()
+
+        members(g, block)
 
     def through_units(g):
         acc_a[...] = jnp.zeros_like(acc_a)
         acc_b[...] = jnp.zeros_like(acc_b)
 
         def body(k, _):
-            @pl.when(k > 0)
-            def _():
-                forwarded(g, k).wait_recv()
-
-            p = (t + k) % n_tp
+            wait_relayed(arrived, arrived_sems, g, k)
+            p = place_of(k)
             part = pl.ds(pl.multiple_of(p * cols, cols), cols)
             rows = arrived[p, group_rows(g)]
             acc_a[...] += jnp.dot(rows, w_gate[part, :], preferred_element_type=jnp.float32)
@@ -305,12 +336,8 @@
 
         lax.fori_loop(0, n_tp, body, 0)
         hidden[t, group_rows(g)] = (jax.nn.silu(acc_a[...]) * acc_b[...]).astype(jnp.bfloat16)
-
-        def send(k, _):
-            hidden_copy(g, k, t).start()
-            return 0
-
-        lax.fori_loop(1, n_tp, send, 0)
+        for i in range(len(direct)):
+            straight(hidden, hidden_sems, g, i, t, group_rows(g)).start()
 
     def give_back(p, q):
         return remote(
@@ -321,12 +348,8 @@
         acc_c[...] = jnp.zeros_like(acc_c)
 
         def body(k, _):
-            p = (t + k) % n_tp
-
-            @pl.when(k > 0)
-            def _():
-                hidden_copy(g, k, p).wait_recv()
-
+            wait_relayed(hidden, hidden_sems, g, k)
+            p = place_of(k)
             part = pl.ds(pl.multiple_of(p * units, units), units)
             acc_c[...] += jnp.dot(
                 hidden[p, group_rows(g)], w_down[part, :], preferred_element_type=jnp.float32
@@ -337,27 +360,38 @@
         result[group_rows(g)] = acc_c[...].astype(jnp.bfloat16)
         others(g, lambda p: give_back(p, s).start())
 
-    for g in ORDER:
-        through_units(g)
-    for g in ORDER:
-        through_down(g)
+    for step in range(GROUPS + 4):
+        for late, action in enumerate(
+            (
+                forward,
+                lambda g: relay(arrived, arrived_sems, g),
+                through_units,
+                lambda g: relay(hidden, hidden_sems, g),
+                through_down,
+            )
+        ):
+            if 0 <= step - late < GROUPS:
+                if late == 2 and step == 2:
+                    for load in loads:
+                        load.wait()
+                action(step - late)
     returned[rows_of(s)] = result[rows_of(s)]
-    for g in range(2):
+    for g in range(GROUPS):
         others(g, lambda p: give_back(p, p).wait_recv())
     out_ref[...] = returned[...]
-    for g in range(2):
+    for g in range(GROUPS):
         others(g, lambda p: dispatch(p, s).wait_send())
         others(g, lambda p: give_back(p, s).wait_send())
-
-        def finish(k, _, g=g):
-            forwarded(g, k).wait_send()
-            hidden_copy(g, k, t).wait_send()
-            return 0
-
-        lax.fori_loop(1, n_tp, finish, 0)
-
-
-ORDER = (0, 1)
+        finish_sends(arrived, arrived_sems, g)
+        finish_sends(hidden, hidden_sems, g)
+
+
+GROUPS = 4
+
+
+def grid_of(count):
+    across = max(k for k in range(1, count + 1) if count % k == 0 and k * k <= count)
+    return across, count // across
 
 
 def through_experts(stream, gain, select, w_gate, w_up, w_down, n_sp, n_tp):
@@ -366,6 +400,8 @@
     width, units = w_gate.shape[1:]
     bf16, f32 = jnp.bfloat16, jnp.float32
     dma = pltpu.SemaphoreType.DMA
+    across, down = grid_of(n_tp)
+    straights, relays = across + down - 2, (across - 1) * (down - 1)
     vmem = pl.BlockSpec(memory_space=pltpu.VMEM)
     hbm = pl.BlockSpec(memory_space=pl.ANY)
     return pl.pallas_call(
@@ -383,18 +419,22 @@
             pltpu.VMEM((n_tp, slots, units), bf16),
             pltpu.VMEM((slots, cols), bf16),
             pltpu.VMEM((slots, cols), bf16),
-            pltpu.VMEM((slots // 2, units), f32),
-            pltpu.VMEM((slots // 2, units), f32),
-            pltpu.VMEM((slots // 2, cols), f32),
+            pltpu.VMEM((slots // GROUPS, units), f32),
+            pltpu.VMEM((slots // GROUPS, units), f32),
+            pltpu.VMEM((slots // GROUPS, cols), f32),
             dma((3,)),
             dma((n_tp,)),
             dma((n_tp,)),
             dma((n_sp,)),
             dma((n_sp,)),
-            dma((2, n_tp)),
-            dma((2, n_tp)),
-            dma((2, n_tp)),
-            dma((2, n_tp)),
+            dma((GROUPS, straights)),
+            dma((GROUPS, n_tp)),
+            dma((GROUPS, 2, relays)),
+            dma((GROUPS, n_tp, 2)),
+            dma((GROUPS, straights)),
+            dma((GROUPS, n_tp)),
+            dma((GROUPS, 2, relays)),
+            dma((GROUPS, n_tp, 2)),
             dma((n_sp,)),
             dma((n_sp,)),
         ],

time: 213 us -> 202 us (0.948)
  Pallas kernels: 125 us -> 113 us
    pallas_call x1, Pallas kernels: 105 us -> 92.2 us  [through_experts(): pl.pallas_call(experts_kernel, out_shape=jax.ShapeDtypeStruct((slots, col...]
where the time goes in v2:
time: 202 us; the launch traced here: 200 us
  Pallas kernels  113 us (56%)
  waiting for transfers between devices  47.6 us (24%)
  between operations  13.9 us (7%)
  matrix products  11.1 us (5%)
  local copies, waits for them, and re-layouts  9.01 us (4%)
  other arithmetic  5.92 us (3%)
    pallas_call x1, Pallas kernels, through_experts(): pl.pallas_call(experts_kernel, out_shape=jax.ShapeDtypeStruct((slots, col...  92.2 us
    all_gather x1, waiting for transfers between devices, per_device(): weight = lax.all_gather(out_weight, 'sp', axis=1, tiled=True)  46.9 us
    pallas_call x1, Pallas kernels, gather_heads(): pl.pallas_call(gather_kernel, out_shape=jax.ShapeDtypeStruct(whole, part....  12.4 us
    pallas_call x1, Pallas kernels, entering_states(): pl.pallas_call(chain_kernel, out_shape=jax.ShapeDtypeStruct(update.shape,...  8.07 us
    unnamed x40, local copies, waits for them, and re-layouts  4.55 us
  transfers between devices with their start and end apart: 1, of which 1 were waited for; matrix products, arithmetic and copies ran while one was open for 9% of the time, Pallas kernels for 10%

profile of v2, /device:TPU:0, one launch (start us, length us, event | category | flops | bytes accessed | tf_op | source)
XLA Modules:
  0.0 200.2 jit_solution(6584012079770270556)
XLA Ops:
  6.5 0.7 all-gather.2.cloned.1.call-update
  7.3 0.8 copy.156
  8.3 1.1 copy.131
  9.8 1.1 copy.145
  11.6 0.7 fusion.70
  12.3 0.4 fusion.64
  14.5 0.6 copy.125
  15.2 0.4 fusion.63
  17.1 0.8 multiply_subtract_fusion
  17.9 0.4 fusion.20
  18.3 1.0 pad_maximum_fusion.update_ref
  19.3 0.7 broadcast_in_dim.39.fall_ref
  20.0 8.1 %shard_map.154 = bf16[12,128,128]{2,1,0:T(8,128)(2,1)} custom-call(f32[12,128,128]{2,1,0:T(8,128)} %pad_maximum_fusion.update_ref, f32[12,1,128]{2,1,0:T(1,128)} %broadcast_in_dim.39.fall_ref), custom_call_target="tpu_custom_call" | custom-call | tf_op jit(solution)/shard_map/pallas_call | solution.py:89
  28.1 1.1 convolution_bitcast_fusion.3
  29.3 1.2 multiply_reduce_fusion.1
  31.1 0.4 convolution_bitcast_fusion.2
  32.1 0.7 pad_maximum_fusion.2.part_ref
  32.8 12.4 %shard_map.155 = bf16[2,128,2048]{2,1,0:T(8,128)(2,1)} custom-call(bf16[2,128,512]{2,1,0:T(8,128)(2,1)} %pad_maximum_fusion.2.part_ref), custom_call_target="tpu_custom_call" | custom-call | tf_op jit(solution)/shard_map/pallas_call | solution.py:130
  45.2 0.6 reduce-window.6
  46.8 46.9 %all-gather.2.cloned.1.call-done = bf16[2,2048,1024]{2,1,0:T(8,128)(2,1)} async-done(((bf16[2,256,1024]{2,1,0:T(8,128)(2,1)}), bf16[2,2048,1024]{2,1,0:T(8,128)(2,1)}) %all-gather.2.cloned.1.call-update) | async-done | bytes 8388624 | tf_op jit(solution)/shard_map/all_gather | solution.py:558
  93.7 3.1 %fusion = f32[128,1024]{1,0:T(8,128)S(1)} fusion(bf16[2,2048,1024]{2,1,0:T(8,128)(2,1)} %all-gather.2.cloned.1.call-done, bf16[2,128,2048]{2,1,0:T(8,128)(2,1)} %shard_map.155), kind=kOutput, calls=%fused_computation.1 | convolution fusion | flops 536870912 | bytes 5242880 | tf_op jit(solution)/shard_map/dot_general | solution.py:561
  96.8 3.0 %fusion.7.stream_ref = f32[128,1024]{1,0:T(8,128)S(1)} fusion(f32[128,1024]{1,0:T(8,128)S(1)} %fusion, bf16[2,2048,1024]{2,1,0:T(8,128)(2,1)} %all-gather.2.cloned.1.call-done, bf16[2,128,2048]{2,1,0:T(8,128)(2,1)S(1)} %copy-done.1, bf16[128,1024]{1,0:T(8,128)(2,1)S(1)} %copy-done.12), kind=kOutput, calls=%fused_computation.11 | convolution fusion | flops 537526272 | bytes 6029312 | tf_op jit(solution)/shard_map/dot_general | solution.py:560
  99.8 92.2 %shard_map.156 = bf16[512,1024]{1,0:T(8,128)(2,1)S(1)} custom-call(f32[128,1024]{1,0:T(8,128)S(1)} %fusion.7.stream_ref, f32[1,1024]{1,0:T(1,128)S(1)} %bitcast.98, bf16[512,128]{1,0:T(8,128)(2,1)S(1)} %convert_bitcast_fusion.select_ref, bf16[1,4096,512]{2,1,0:T(8,128)(2,1)} %gate_hbm.1, bf16[1,4096,512]{2,1,0:T(8,128)(2,1)} %up_hbm.1, ...), custom_call_target="tpu_custom_call" | custom-call | tf_op jit(solution)/shard_map/pallas_call | solution.py:407
  192.3 1.0 fusion.8
  (99 shorter events, 7.0 us)
Async XLA Ops:
  6.5 4.7 %copy-start.9 = (f32[128,2,4]{0,2,1:T(4,128)S(1)}, f32[128,2,4]{0,2,1:T(4,128)}, u32[]{:S(2)}) copy-start(f32[128,2,4]{0,2,1:T(4,128)} %param.23) | copy-start | bytes 12292
  6.5 5.8 %copy-start.2 = (bf16[128,2,512]{2,1,0:T(2,128)(2,1)S(1)}, bf16[128,2,512]{2,1,0:T(2,128)(2,1)}, u32[]{:S(2)}) copy-start(bf16[128,2,512]{2,1,0:T(2,128)(2,1)} %param.21) | copy-start | bytes 786436
  6.5 6.3 %copy-start.6 = (bf16[128,512]{1,0:T(8,128)(2,1)S(1)}, bf16[128,512]{1,0:T(8,128)(2,1)}, u32[]{:S(2)}) copy-start(bf16[128,512]{1,0:T(8,128)(2,1)} %param.17) | copy-start | bytes 393220
  6.5 87.2 %all-gather.2.cloned.1.call-start = ((), (), s32[]{:S(2)}) async-start(), calls=%async_computation | async-start | bytes 9437184 | tf_op jit(solution)/shard_map/all_gather | solution.py:558
  9.5 3.8 %copy-start.7 = (bf16[128,512]{1,0:T(8,128)(2,1)S(1)}, bf16[128,512]{1,0:T(8,128)(2,1)}, u32[]{:S(2)}) copy-start(bf16[128,512]{1,0:T(8,128)(2,1)} %param.18) | copy-start | bytes 393220
  10.9 4.3 %copy-start.3 = (bf16[128,2,512]{2,1,0:T(2,128)(2,1)S(1)}, bf16[128,2,512]{2,1,0:T(2,128)(2,1)}, u32[]{:S(2)}) copy-start(bf16[128,2,512]{2,1,0:T(2,128)(2,1)} %param.22) | copy-start | bytes 786436
  17.9 12.6 %copy-start.10 = (f32[2,512]{1,0:T(2,128)S(1)}, f32[2,512]{1,0:T(2,128)}, u32[]{:S(2)}) copy-start(f32[2,512]{1,0:T(2,128)} %param.24) | copy-start | bytes 12292
  17.9 12.9 %copy-start.5 = (f32[128,4]{1,0:T(8,128)S(1)}, f32[128,4]{1,0:T(8,128)}, u32[]{:S(2)}) copy-start(f32[128,4]{1,0:T(8,128)} %get-tuple-element.31) | copy-start | bytes 6148
  17.9 13.2 %copy-start.4 = (bf16[128,4,128]{2,0,1:T(8,128)(2,1)S(1)}, bf16[128,4,128]{2,0,1:T(8,128)(2,1)}, u32[]{:S(2)}) copy-start(bf16[128,4,128]{2,0,1:T(8,128)(2,1)} %get-tuple-element.28) | copy-start | bytes 393220
  28.1 3.4 %slice-start = ((bf16[12,128,128]{2,1,0:T(8,128)(2,1)}), bf16[8,128,128]{2,1,0:T(8,128)(2,1)S(1)}, s32[]{:S(2)}) async-start(bf16[12,128,128]{2,1,0:T(8,128)(2,1)} %shard_map.154), calls=%async_computation.1 | async-start | bytes 524288 | tf_op jit(solution)/shard_map/slice | solution.py:554
  29.3 17.1 %copy-start.8 = (s32[128,2]{0,1:T(2,128)S(1)}, s32[128,2]{0,1:T(2,128)}, u32[]{:S(2)}) copy-start(s32[128,2]{0,1:T(2,128)} %param.27) | copy-start | bytes 3076
  30.5 16.1 %copy-start.11 = (f32[128,2]{0,1:T(2,128)S(1)}, f32[128,2]{0,1:T(2,128)}, u32[]{:S(2)}) copy-start(f32[128,2]{0,1:T(2,128)} %param.28) | copy-start | bytes 3076
  45.2 51.6 %copy-start.1 = (bf16[2,128,2048]{2,1,0:T(8,128)(2,1)S(1)}, bf16[2,128,2048]{2,1,0:T(8,128)(2,1)}, u32[]{:S(2)}) copy-start(bf16[2,128,2048]{2,1,0:T(8,128)(2,1)} %shard_map.155) | copy-start | bytes 3145732
  45.2 51.6 %copy-start.12 = (bf16[128,1024]{1,0:T(8,128)(2,1)S(1)}, bf16[128,1024]{1,0:T(8,128)(2,1)}, u32[]{:S(2)}) copy-start(bf16[128,1024]{1,0:T(8,128)(2,1)} %param.16) | copy-start | bytes 786436
  96.8 3.0 %copy-start = (f32[1024]{0:T(1024)S(1)}, f32[1024]{0:T(1024)}, u32[]{:S(2)}) copy-start(f32[1024]{0:T(1024)} %param.26) | copy-start | bytes 12292
Sparse Core Ops, SparseCore 0:
  8.9 84.7 all-gather.1
